TPU v7x, 32 devices: a whole 2x2x4 slice. The times are simulated.
32 devices in a mesh: sp: 8 (over z, x), tp: 4 (over y, core).
Axes of the slice: x: 2, y: 2, z: 4, core: 2. Of those that a mesh axis runs over, the one named last changes fastest.
Arguments:
- lane_source_signal: bfloat16 [1024, 1024], P('tp', 'sp'), may hold values from -6 to 6
- spectral_damping_part: float32 [64, 64], P('tp'), may hold values from -3 to -0.0002
- spectral_angular_part: float32 [64, 64], P('tp'), may hold values from 0.31 to 201.0624
- interval_exponent: float32 [64], P('tp'), may hold values from -3.9 to -1.6
- entry_matrix_inphase: float32 [64, 64, 16], P('tp'), may hold values from -1 to 1
- entry_matrix_quadrature: float32 [64, 64, 16], P('tp'), may hold values from -1 to 1
- emission_inphase: float32 [64, 16, 64], P('tp'), may hold values from -0.75 to 0.75
- emission_quadrature: float32 [64, 16, 64], P('tp'), may hold values from -0.75 to 0.75
- lane_bypass_factor: float32 [1024], P('tp'), may hold values from -5 to 5
- spike_shrink_offset: float32 [64, 1024], P('tp', 'sp'), may hold values from -1.4 to 0
- lane_exit_matrix: bfloat16 [1024, 4096], P('tp'), may hold values from -0.1875 to 0.1875
- skipline_stream: bfloat16 [1024, 4096], P('sp'), may hold values from -6 to 6
- specialist_scaling_vector: float32 [4096], replicated, may hold values from 0.1 to 1.9
- selected_specialists: int32 [1024, 2], P('sp'), may hold values from 0 to 7, all different within a row; in each aligned block of 128 rows (0 to 127, 128 to 255, ...) at most 64 rows name the same one
- dispatcher_scores: float32 [1024, 2], P('sp'), may hold values from 0.1 to 1
- specialist_valve_matrix: bfloat16 [8, 4096, 2048], P('sp', None, 'tp'), may hold values from -0.09375 to 0.09375
- specialist_widen_matrix: bfloat16 [8, 4096, 2048], P('sp', None, 'tp'), may hold values from -0.09375 to 0.09375
- specialist_shrink_matrix: bfloat16 [8, 2048, 4096], P('sp', 'tp'), may hold values from -0.1875 to 0.1875
Outputs:
- updated: bfloat16 [1024, 4096], P('sp', 'tp')
Inputs may be any that keep to these rules, and one draw needn't show every extreme that they name: `selected_specialists`: each row names 2 different experts. Among the rows of each aligned block of 128 positions no expert is named more than 64 times, and in every block some expert is named exactly 64 times.
All inputs are finite; a program needn't handle non-finite values.
Results may differ from a plain program's by a relative error of at most 0.019.
Values may be sent and summed in bfloat16 or wider, within the bound.
A program may use at most 64 MiB of HBM per device.

v0:
```python
import jax
import jax.numpy as jnp
from jax import lax
from jax.sharding import PartitionSpec as P

EPS = 1e-06
PRECISE_MODE = lax.Precision.HIGHEST


def carried_in(value, axis, join, neutral):
    count, mine = (lax.axis_size(axis), lax.axis_index(axis))
    pieces = jax.tree.map(lambda part: lax.all_gather(part, axis), value)
    running = jax.tree.map(
        lambda part, zero: jnp.full_like(part, 0) + jnp.asarray(zero, part.dtype), value, neutral
    )

    def lap(position, running):
        longer = join(running, jax.tree.map(lambda part: part[position], pieces))
        return jax.tree.map(lambda new, old: jnp.where(position < mine, new, old), longer, running)

    return lax.fori_loop(0, count - 1, lap, running)


def affine_pair(earlier, latter):
    mul_re = earlier[0] * latter[0] - earlier[1] * latter[1]
    mul_im = earlier[0] * latter[1] + earlier[1] * latter[0]
    add_re = latter[0] * earlier[2] - latter[1] * earlier[3] + latter[2]
    add_im = latter[0] * earlier[3] + latter[1] * earlier[2] + latter[3]
    return (mul_re, mul_im, add_re, add_im)


def local_prefix(elements):
    length = elements[0].shape[2]
    fills = (1.0, 0.0, 0.0, 0.0)
    offset = 1
    while offset < length:
        earlier = tuple(
            (
                jnp.pad(
                    item[:, :, : length - offset],
                    ((0, 0), (0, 0), (offset, 0)),
                    constant_values=fill,
                )
                for item, fill in zip(elements, fills)
            )
        )
        elements = affine_pair(earlier, elements)
        offset = offset * 2
    return elements


def full_norm(projected, skipline_stream, specialist_scaling_vector, col_start, d_local):
    stream = (
        skipline_stream.astype(jnp.float32)
        + lax.optimization_barrier(projected).astype(jnp.float32)
    ).astype(jnp.bfloat16)
    stream_f = lax.optimization_barrier(stream).astype(jnp.float32)
    inv_rms = lax.rsqrt(jnp.mean(stream_f * stream_f, axis=-1, keepdims=True) + EPS)
    normed = (stream_f * inv_rms * specialist_scaling_vector).astype(jnp.bfloat16)
    own_stream = lax.dynamic_slice_in_dim(stream_f, col_start, d_local, 1)
    own_cols = lax.dynamic_slice_in_dim(normed, col_start, d_local, 1)
    return (own_stream, normed, own_cols)


def per_device(
    lane_source_signal,
    spectral_damping_part,
    spectral_angular_part,
    interval_exponent,
    entry_matrix_inphase,
    entry_matrix_quadrature,
    emission_inphase,
    emission_quadrature,
    lane_bypass_factor,
    spike_shrink_offset,
    lane_exit_matrix,
    skipline_stream,
    specialist_scaling_vector,
    selected_specialists,
    dispatcher_scores,
    specialist_valve_matrix,
    specialist_widen_matrix,
    specialist_shrink_matrix,
):
    f32 = jnp.float32
    bf16 = jnp.bfloat16
    groups_here = spectral_damping_part.shape[0]
    lanes_within_bundle = entry_matrix_inphase.shape[2]
    tok_local = lane_source_signal.shape[1]
    bundled_signal = lane_source_signal.astype(f32).reshape(
        groups_here, lanes_within_bundle, tok_local
    )
    step_size = jnp.exp(interval_exponent)[:, None]
    natural_pace_exponent = spectral_damping_part * step_size
    angle = spectral_angular_part * step_size
    num_re = jnp.expm1(natural_pace_exponent) * jnp.cos(angle) - 2.0 * jnp.sin(0.5 * angle) ** 2
    num_im = jnp.exp(natural_pace_exponent) * jnp.sin(angle)
    denom = (
        spectral_damping_part * spectral_damping_part
        + spectral_angular_part * spectral_angular_part
    )
    fac_re = (num_re * spectral_damping_part + num_im * spectral_angular_part) / denom
    fac_im = (num_im * spectral_damping_part - num_re * spectral_angular_part) / denom
    map_re = (
        fac_re[:, :, None] * entry_matrix_inphase - fac_im[:, :, None] * entry_matrix_quadrature
    )
    map_im = (
        fac_re[:, :, None] * entry_matrix_quadrature + fac_im[:, :, None] * entry_matrix_inphase
    )
    drive_re = jnp.einsum("gpc,gct->gpt", map_re, bundled_signal, precision=PRECISE_MODE)
    drive_im = jnp.einsum("gpc,gct->gpt", map_im, bundled_signal, precision=PRECISE_MODE)
    recurrence_modulus = jnp.exp(
        natural_pace_exponent[:, :, None] + spike_shrink_offset[:, None, :]
    )
    trans_re = recurrence_modulus * jnp.cos(angle)[:, :, None]
    trans_im = recurrence_modulus * jnp.sin(angle)[:, :, None]
    cum_re, cum_im, state_real, state_imaginary = local_prefix(
        (trans_re, trans_im, drive_re, drive_im)
    )
    summary = (cum_re[:, :, -1], cum_im[:, :, -1], state_real[:, :, -1], state_imaginary[:, :, -1])
    unit = jnp.ones_like(summary[0])
    blank = jnp.zeros_like(summary[0])
    carried = carried_in(summary, "sp", affine_pair, (unit, blank, blank, blank))
    enter_re = carried[2][:, :, None]
    enter_im = carried[3][:, :, None]
    state_real = state_real + cum_re * enter_re - cum_im * enter_im
    state_imaginary = state_imaginary + cum_re * enter_im + cum_im * enter_re
    value = (
        jnp.einsum("nef,nfi->nei", emission_inphase, state_real, precision=PRECISE_MODE)
        - jnp.einsum("nef,nfi->nei", emission_quadrature, state_imaginary, precision=PRECISE_MODE)
        + lane_bypass_factor.reshape(groups_here, lanes_within_bundle)[:, :, None] * bundled_signal
    )
    recurrence_result = (
        jax.nn.gelu(value).astype(bf16).reshape(groups_here * lanes_within_bundle, tok_local)
    )
    width = specialist_scaling_vector.shape[0]
    d_local = width // lax.axis_size("tp")
    col_start = lax.axis_index("tp") * d_local
    partial_rows = jnp.einsum(
        "ct,cd->td", recurrence_result, lane_exit_matrix, preferred_element_type=f32
    )
    projected = lax.psum(partial_rows.astype(jnp.bfloat16), "tp").astype(jnp.float32).astype(bf16)
    own_stream, normed, own_cols = full_norm(
        projected, skipline_stream, specialist_scaling_vector, col_start, d_local
    )
    share = dispatcher_scores / jnp.sum(dispatcher_scores, axis=1, keepdims=True)
    experts = lax.axis_size("sp")
    top = selected_specialists.shape[1]
    capacity = 2 * tok_local * top // experts
    flat_routes = selected_specialists.reshape(-1)
    hits = (flat_routes[:, None] == jnp.arange(experts, dtype=jnp.int32)[None, :]).astype(jnp.int32)
    ranks = jnp.sum((jnp.cumsum(hits, axis=0) - hits) * hits, axis=1)
    slot_ids = flat_routes * capacity + ranks
    slot_grid = jnp.arange(experts * capacity, dtype=jnp.int32)
    matched = slot_grid[:, None] == slot_ids[None, :]
    token_of = jnp.arange(tok_local * top, dtype=jnp.int32) // top
    slot_token = jnp.sum(jnp.where(matched, token_of[None, :], 0), axis=1)
    slot_live = jnp.any(matched, axis=1)
    gate_w = specialist_valve_matrix[0]
    up_w = specialist_widen_matrix[0]
    down_w = specialist_shrink_matrix[0]
    bf_zero = jnp.zeros((), bf16)
    dispatch = jnp.where(slot_live[:, None], own_cols[slot_token], bf_zero).reshape(
        experts, capacity, d_local
    )
    arrived = lax.all_to_all(dispatch, "sp", split_axis=0, concat_axis=0, tiled=True)
    piece = lax.all_gather(arrived, "tp", axis=2, tiled=True)
    gate_part = jnp.einsum("snd,df->snf", piece, gate_w, preferred_element_type=f32)
    up_part = jnp.einsum("snd,df->snf", piece, up_w, preferred_element_type=f32)
    hidden = (jax.nn.silu(gate_part) * up_part).astype(bf16)
    flat_hidden = hidden.reshape(experts * capacity, hidden.shape[2])
    down_part = jnp.dot(flat_hidden, down_w, preferred_element_type=f32).astype(bf16)
    summed = lax.psum_scatter(
        down_part.astype(f32).astype(jnp.bfloat16), "tp", scatter_dimension=1, tiled=True
    ).astype(jnp.float32)
    expert_out = summed.astype(bf16).reshape(experts, capacity, d_local)
    returned = lax.all_to_all(expert_out, "sp", split_axis=0, concat_axis=0, tiled=True).reshape(
        experts * capacity, d_local
    )
    picked = returned[slot_ids].reshape(tok_local, top, d_local)
    combined = jnp.sum(lax.optimization_barrier(picked).astype(f32) * share[:, :, None], axis=1)
    return (own_stream + combined).astype(bf16)


def solution(mesh):
    placed = (
        P("tp", "sp"),
        P("tp", None),
        P("tp", None),
        P("tp"),
        P("tp", None, None),
        P("tp", None, None),
        P("tp", None, None),
        P("tp", None, None),
        P("tp"),
        P("tp", "sp"),
        P("tp", None),
        P("sp", None),
        P(),
        P("sp", None),
        P("sp", None),
        P("sp", None, "tp"),
        P("sp", None, "tp"),
        P("sp", "tp", None),
    )
    return jax.shard_map(
        per_device, mesh=mesh, in_specs=placed, out_specs=P("sp", "tp"), check_vma=False
    )
```

profile of v0, /device:TPU:11, one launch (start us, length us, event | category | flops | bytes accessed | tf_op | source)
XLA Modules:
  0.0 366.0 jit_solution(14271177628407040252)
XLA Ops:
  8.2 1.6 fusion.45
  9.8 1.6 fusion.49
  23.2 21.8 %all-gather = f32[128,64,1]{1,2,0:T(1,128)S(1)} all-gather(f32[16,64,1]{1,2,0:T(1,128)S(1)} %copy.32), channel_id=2, replica_groups=mesh['sp'=8,'tp'=4] {'sp'}, dimensions={0}, use_global_device_ids=true | all-gather | bytes 36864 | tf_op jit(solution)/shard_map/all_gather | solution.py:12
  47.3 24.2 %all-gather.1 = f32[128,64,1]{1,2,0:T(1,128)S(1)} all-gather(f32[16,64,1]{1,2,0:T(1,128)S(1)} %copy.33), channel_id=3, replica_groups=mesh['sp'=8,'tp'=4] {'sp'}, dimensions={0}, use_global_device_ids=true | all-gather | bytes 36864 | tf_op jit(solution)/shard_map/all_gather | solution.py:12
  71.4 2.0 slice.170
  74.7 24.3 %all-gather.2 = f32[128,64,1]{1,2,0:T(1,128)S(1)} all-gather(f32[16,64,1]{1,2,0:T(1,128)S(1)} %copy.34), channel_id=4, replica_groups=mesh['sp'=8,'tp'=4] {'sp'}, dimensions={0}, use_global_device_ids=true | all-gather | bytes 36864 | tf_op jit(solution)/shard_map/all_gather | solution.py:12
  99.0 2.0 slice.171
  102.3 24.0 %all-gather.3 = f32[128,64,1]{1,2,0:T(1,128)S(1)} all-gather(f32[16,64,1]{1,2,0:T(1,128)S(1)} %copy.35), channel_id=5, replica_groups=mesh['sp'=8,'tp'=4] {'sp'}, dimensions={0}, use_global_device_ids=true | all-gather | bytes 36864 | tf_op jit(solution)/shard_map/all_gather | solution.py:12
  126.7 1.9 fusion.22
  128.6 1.9 fusion.42
  130.5 1.5 convolution_convert_fusion.1
  134.0 62.8 %all-reduce.30.cloned.1.call-done = bf16[128,4096]{1,0:T(8,128)(2,1)} async-done(((bf16[128,4096]{1,0:T(8,128)(2,1)}), bf16[128,4096]{1,0:T(8,128)(2,1)}) %all-reduce.30.cloned.1.call-update) | async-done | bytes 1048592 | tf_op jit(solution)/shard_map/psum | solution.py:142
  196.9 1.8 add_convert_fusion
  200.3 2.1 gather_fusion
  202.5 27.8 %all_to_all.10 = bf16[8,64,1024]{2,1,0:T(8,128)(2,1)} all-to-all(bf16[8,64,1024]{2,1,0:T(8,128)(2,1)S(1)} %broadcast_select_fusion), channel_id=1, replica_groups=mesh['sp'=8,'tp'=4] {'sp'}, dimensions={0} | all-to-all | bytes 2097152 | tf_op jit(solution)/shard_map/all_to_all | solution.py:166
  230.3 37.3 %all-gather.6.cloned.1.call-done = bf16[8,64,4096]{2,1,0:T(8,128)(2,1)} async-done(((bf16[8,64,1024]{2,1,0:T(8,128)(2,1)}), bf16[8,64,4096]{2,1,0:T(8,128)(2,1)}) %all-gather.6.cloned.1.call-update) | async-done | bytes 4194320 | tf_op jit(solution)/shard_map/all_gather | solution.py:167
  267.7 5.9 %fusion.7 = f32[8,64,512]{2,1,0:T(8,128)S(1)} fusion(bf16[8,64,4096]{2,1,0:T(8,128)(2,1)} %all-gather.6.cloned.1.call-done, bf16[1,4096,512]{2,1,0:T(8,128)(2,1)} %param.35), kind=kOutput, calls=%fused_computation.17 | convolution fusion | flops 2147483648 | bytes 9437184 | tf_op jit(solution)/shard_map/snd,df->snf/dot_general | solution.py:168
  273.6 2.4 fusion.12
  276.1 4.3 %convolution_convert_fusion = bf16[512,4096]{1,0:T(8,128)(2,1)} fusion(bf16[512,512]{1,0:T(8,128)(2,1)S(1)} %bitcast.169, bf16[1,512,4096]{2,1,0:T(8,128)(2,1)S(1)} %copy-done.8), kind=kOutput, calls=%fused_computation.12 | convolution fusion | flops 2149580800 | bytes 8912896 | tf_op jit(solution)/shard_map/dot_general | solution.py:172
  280.4 44.0 %reduce-scatter.2.cloned.1.call-done = bf16[512,1024]{1,0:T(8,128)(2,1)} async-done(((bf16[512,4096]{1,0:T(8,128)(2,1)}), bf16[512,1024]{1,0:T(8,128)(2,1)}) %reduce-scatter.2.cloned.1.call-update) | async-done | bytes 1048592 | tf_op jit(solution)/shard_map/reduce_scatter | solution.py:173
  324.4 5.5 %all-to-all-start.1 = ((bf16[8,64,1024]{2,1,0:T(8,128)(2,1)}), bf16[8,64,1024]{2,1,0:T(8,128)(2,1)S(1)}, u32[]{:S(2)}, u32[]{:S(2)}) async-start(bf16[8,64,1024]{2,1,0:T(8,128)(2,1)} %bitcast.156), calls=%async_computation.2 | async-start | bytes 2097152 | tf_op jit(solution)/shard_map/all_to_all | solution.py:177
  330.3 22.8 %all-to-all-done.1 = bf16[8,64,1024]{2,1,0:T(8,128)(2,1)S(1)} async-done(((bf16[8,64,1024]{2,1,0:T(8,128)(2,1)}), bf16[8,64,1024]{2,1,0:T(8,128)(2,1)S(1)}, u32[]{:S(2)}, u32[]{:S(2)}) %all-to-all-start.1) | async-done | bytes 1048608 | tf_op jit(solution)/shard_map/all_to_all | solution.py:177
  353.1 2.0 gather_fusion.1
  357.7 1.8 add_convert_fusion.1
  (90 shorter events, 25.5 us)
Async XLA Ops:
  6.5 123.9 %copy-start = (bf16[256,4096]{1,0:T(8,128)(2,1)S(1)}, bf16[256,4096]{1,0:T(8,128)(2,1)}, u32[]{:S(2)}) copy-start(bf16[256,4096]{1,0:T(8,128)(2,1)} %param.30) | copy-start | bytes 6291460
  6.5 6.3 %copy-start.3 = (f32[16,128]{1,0:T(8,128)S(1)}, f32[16,128]{1,0:T(8,128)}, u32[]{:S(2)}) copy-start(f32[16,128]{1,0:T(8,128)} %param.29) | copy-start | bytes 24580
  6.5 190.3 %all-reduce.30.cloned.1.call-start = ((), (), s32[]{:S(2)}) async-start(), calls=%async_computation.3 | async-start | bytes 2097152 | tf_op jit(solution)/shard_map/psum | solution.py:142
  20.9 105.7 %copy-start.6 = (f32[256]{0:T(256)S(1)}, f32[256]{0:T(256)}, u32[]{:S(2)}) copy-start(f32[256]{0:T(256)} %param.28) | copy-start | bytes 3076
  21.9 106.7 %copy-start.2 = (bf16[256,128]{1,0:T(8,128)(2,1)S(1)}, bf16[256,128]{1,0:T(8,128)(2,1)}, u32[]{:S(2)}) copy-start(bf16[256,128]{1,0:T(8,128)(2,1)} %param.20) | copy-start | bytes 196612
  126.6 5.6 %copy-start.4 = (s32[128,2]{0,1:T(2,128)S(1)}, s32[128,2]{0,1:T(2,128)}, u32[]{:S(2)}) copy-start(s32[128,2]{0,1:T(2,128)} %param.33) | copy-start | bytes 3076
  132.0 135.7 %all-gather.6.cloned.1.call-start = ((), (), s32[]{:S(2)}) async-start(), calls=%async_computation.4 | async-start | bytes 5242880 | tf_op jit(solution)/shard_map/all_gather | solution.py:167
  133.9 66.3 %dynamic-slice-start = ((f32[4096]{0:T(1024)}, s32[]{:T(128)}), f32[1024]{0:T(1024)S(1)}, s32[]{:S(2)}) async-start(f32[4096]{0:T(1024)} %param.32, s32[]{:T(128)} %select_n.74), calls=%async_computation.6 | async-start | bytes 8704 | tf_op jit(solution)/shard_map/dynamic_slice | solution.py:61
  198.9 1.3 copy-start.1
  230.3 94.1 %reduce-scatter.2.cloned.1.call-start = ((), (), s32[]{:S(2)}) async-start(), calls=%async_computation.5 | async-start | bytes 5242880 | tf_op jit(solution)/shard_map/reduce_scatter | solution.py:173
  267.7 5.9 %copy-start.7 = (bf16[1,4096,512]{2,1,0:T(8,128)(2,1)S(1)}, bf16[1,4096,512]{2,1,0:T(8,128)(2,1)}, u32[]{:S(2)}) copy-start(bf16[1,4096,512]{2,1,0:T(8,128)(2,1)} %param.36) | copy-start | bytes 12582916
  267.7 5.9 %copy-start.9 = (bf16[8,64,4096]{2,1,0:T(8,128)(2,1)S(1)}, bf16[8,64,4096]{2,1,0:T(8,128)(2,1)}, u32[]{:S(2)}) copy-start(bf16[8,64,4096]{2,1,0:T(8,128)(2,1)} %all-gather.6.cloned.1.call-done) | copy-start | bytes 12582916
  273.6 2.5 copy-start.8
  280.4 49.8 %copy-start.5 = (f32[128,2]{0,1:T(2,128)S(1)}, f32[128,2]{0,1:T(2,128)}, u32[]{:S(2)}) copy-start(f32[128,2]{0,1:T(2,128)} %param.34) | copy-start | bytes 3076
  324.4 28.7 %all-to-all-start.1 = ((bf16[8,64,1024]{2,1,0:T(8,128)(2,1)}), bf16[8,64,1024]{2,1,0:T(8,128)(2,1)S(1)}, u32[]{:S(2)}, u32[]{:S(2)}) async-start(bf16[8,64,1024]{2,1,0:T(8,128)(2,1)} %bitcast.156), calls=%async_computation.2 | async-start | bytes 2097152 | tf_op jit(solution)/shard_map/all_to_all | solution.py:177
Sparse Core Ops, SparseCore 0:
  132.1 64.6 all-reduce.29
  230.4 37.1 all-gather.5
  280.5 43.8 reduce-scatter.1
where the time goes:
time: 371 us; the launch traced here: 366 us
  waiting for transfers between devices  167 us (45%)
  blocking collectives  122 us (33%)
  matrix products  21 us (6%)
  local copies, waits for them, and re-layouts  19.4 us (5%)
  other arithmetic  17.3 us (5%)
  between operations  13.5 us (4%)
  starting transfers between devices  5.75 us (2%)
    all_gather x4, blocking collectives, carried_in(): pieces = jax.tree.map(lambda part: lax.all_gather(part, axis), value)  94.3 us
    psum x1, waiting for transfers between devices, per_device(): lax.psum(partial_rows.astype(jnp.bfloat16), 'tp').astype(jnp.float32)  62.8 us
    reduce_scatter x1, waiting for transfers between devices, per_device(): lax.psum_scatter(down_part.astype(f32).astype(jnp.bfloat16), 'tp', scatte...  44 us
    all_gather x1, waiting for transfers between devices, per_device(): piece = lax.all_gather(arrived, 'tp', axis=2, tiled=True)  37.3 us
    all_to_all x1, blocking collectives, per_device(): lax.all_to_all(dispatch, 'sp', split_axis=0, concat_axis=0, tiled=True)  27.8 us
    all_to_all x1, waiting for transfers between devices, per_device(): lax.all_to_all(expert_out, 'sp', split_axis=0, concat_axis=0, tiled=True)  22.8 us
  transfers between devices with their start and end apart: 4, of which 4 were waited for; matrix products, arithmetic and copies ran while one was open for 1% of the time, Pallas kernels for 0%

commit v1 on v0

v1 whole, which is shorter than its diff:
```python
import jax
import jax.numpy as jnp
from jax import lax
from jax.experimental import pallas as pl
from jax.experimental.pallas import tpu as pltpu
from jax.sharding import PartitionSpec as P

EPS = 1e-06
PRECISE_MODE = lax.Precision.HIGHEST


MESH = pl.DeviceIdType.MESH
VM = pl.BlockSpec(memory_space=pltpu.VMEM)
DMA = pltpu.SemaphoreType.DMA
VMEM_ROOM = 60 * 1024 * 1024


def greet(peers):
    barrier = pltpu.get_barrier_semaphore()
    for peer in peers:
        pl.semaphore_signal(barrier, inc=1, device_id=peer, device_id_type=MESH)
    pl.semaphore_wait(barrier, len(peers))


def remote(src, dst, send, recv, where):
    return pltpu.make_async_remote_copy(
        src_ref=src, dst_ref=dst, send_sem=send, recv_sem=recv, device_id=where, device_id_type=MESH
    )


def places():
    n_sp, n_tp = lax.axis_size("sp"), lax.axis_size("tp")
    return n_sp, n_tp, lax.axis_index("sp"), lax.axis_index("tp")


def carry_kernel(mine, out, pieces, send, recv):
    n_sp, n_tp, me, lane = places()
    greet([(lax.rem(me + i, n_sp), lane) for i in range(1, n_sp)])
    copies = []
    for i in range(1, n_sp):
        copy = remote(
            mine, pieces.at[i - 1], send.at[i - 1], recv.at[i - 1], (lax.rem(me + i, n_sp), lane)
        )
        copy.start()
        copies.append(copy)
    for copy in copies:
        copy.wait_recv()
    run_re = jnp.zeros(mine.shape[1:], jnp.float32)
    run_im = run_re
    for i in range(n_sp - 1, 0, -1):
        mul_re, mul_im, add_re, add_im = (pieces[i - 1, plane] for plane in range(4))
        new_re = mul_re * run_re - mul_im * run_im + add_re
        new_im = mul_re * run_im + mul_im * run_re + add_im
        run_re = jnp.where(me >= i, new_re, run_re)
        run_im = jnp.where(me >= i, new_im, run_im)
    out[0] = run_re
    out[1] = run_im
    for copy in copies:
        copy.wait_send()


def carry_call(summary):
    n_sp = lax.axis_size("sp")
    return pl.pallas_call(
        carry_kernel,
        out_shape=jax.ShapeDtypeStruct((2,) + summary.shape[1:], jnp.float32),
        in_specs=[VM],
        out_specs=VM,
        scratch_shapes=[
            pltpu.VMEM((n_sp - 1,) + summary.shape, jnp.float32),
            DMA((n_sp - 1,)),
            DMA((n_sp - 1,)),
        ],
        compiler_params=pltpu.CompilerParams(collective_id=0, has_side_effects=True),
        name="carry",
    )(summary)


def tp_peers(n_tp, me, lane):
    return [(me, lax.rem(lane + i, n_tp)) for i in range(1, n_tp)]


def sp_peers(n_sp, me, lane):
    return [(lax.rem(me + i, n_sp), lane) for i in range(1, n_sp)]


def dispatch_kernel(
    rows, w, skip, gain, hot,
    stream_out, xs,
    psend, precv, ysend, yrecv, ssend, srecv, dsend,
    ps, pr, ys, yr, ss, sr, ds, dr, fs, fr, qs, qr,
):
    f32, bf16 = jnp.float32, jnp.bfloat16
    n_sp, n_tp, me, lane = places()
    n_y = n_tp // 2
    y, core = lane // 2, lax.rem(lane, 2)
    partner = (me, y * 2 + 1 - core)
    d_local = stream_out.shape[1]
    cap = hot.shape[0] // n_sp
    greet(tp_peers(n_tp, me, lane) + sp_peers(n_sp, me, lane))

    def cols(block):
        return pl.ds(pl.multiple_of(block * d_local, 128), d_local)

    def rows_of(source):
        return pl.ds(pl.multiple_of(source * cap, 16), cap)

    def part(block):
        return jnp.dot(rows[...], w[:, cols(block)], preferred_element_type=f32)

    def y_at(i):
        return lax.rem(y + i, n_y)

    waits = []

    def go(copy):
        copy.start()
        waits.append(copy)
        return copy

    pair = []
    for i in range(n_y - 1, -1, -1):
        psend[i] = part(y_at(i) * 2 + 1 - core).astype(bf16)
        pair.append(go(remote(psend.at[i], precv.at[i], ps.at[i], pr.at[i], partner)))
    pair = pair[::-1]
    across = []
    for i in range(n_y - 1, 0, -1):
        own = part(y_at(i) * 2 + core)
        pair[i].wait_recv()
        ysend[i - 1] = (own + precv[i].astype(f32)).astype(bf16)
        across.append(
            go(
                remote(
                    ysend.at[i - 1], yrecv.at[i - 1], ys.at[i - 1], yr.at[i - 1],
                    (me, y_at(i) * 2 + core),
                )
            )
        )
    total = part(lane)
    pair[0].wait_recv()
    total = total + precv[0].astype(f32)
    for i, copy in enumerate(across[::-1]):
        copy.wait_recv()
        total = total + yrecv[i].astype(f32)
    projected = total.astype(bf16).astype(f32)
    stream = (skip[:, cols(lane)].astype(f32) + projected).astype(bf16)
    stream_out[...] = stream
    stream_f = stream.astype(f32)
    tok = stream_f.shape[0]
    square = jnp.sum(stream_f * stream_f, axis=1, keepdims=True)
    as_rows = jnp.broadcast_to(square, (tok, 128)).T[0:8, :]
    ssend[...] = as_rows
    sums = []
    for i in range(1, n_tp):
        sums.append(
            go(
                remote(
                    ssend, srecv.at[i - 1], ss.at[i - 1], sr.at[i - 1], (me, lax.rem(lane + i, n_tp))
                )
            )
        )
    for i, copy in enumerate(sums):
        copy.wait_recv()
        as_rows = as_rows + srecv[i]
    width = n_tp * d_local
    inv = lax.rsqrt(as_rows / width + EPS)
    inv_rms = jnp.broadcast_to(inv[0:1, :], (128, tok)).T[:, 0:1]
    normed = (stream_f * inv_rms * gain[0:1, cols(lane)]).astype(bf16)

    out_cols = cols(lane)
    arrivals = []
    for i in range(1, n_sp):
        to = lax.rem(me + i, n_sp)
        dsend[i - 1] = jnp.dot(hot[rows_of(to), :], normed, preferred_element_type=f32).astype(bf16)
        arrivals.append(
            go(
                remote(
                    dsend.at[i - 1], xs.at[rows_of(me), out_cols], ds.at[i - 1], dr.at[i - 1],
                    (to, lane),
                )
            )
        )
    xs[rows_of(me), out_cols] = jnp.dot(
        hot[rows_of(me), :], normed, preferred_element_type=f32
    ).astype(bf16)

    def spread(n, source):
        there = xs.at[rows_of(source), out_cols]
        for i in range(1, n_y):
            k = (i - 1) * n_sp + n
            go(remote(there, there, fs.at[k], fr.at[k], (me, y_at(i) * 2 + core)))
        go(remote(there, there, qs.at[n], qr.at[n], partner))

    def source_at(n):
        return lax.rem(me + n_sp - n, n_sp)

    def landed(source, block, recv, send):
        here = xs.at[rows_of(source), cols(block)]
        remote(here, here, send, recv, partner).wait_recv()

    spread(0, me)
    for n in range(1, n_sp):
        landed(source_at(n), lane, dr.at[n - 1], ds.at[n - 1])
        spread(n, source_at(n))
    for n in range(n_sp):
        for i in range(1, n_y):
            k = (i - 1) * n_sp + n
            from_block = lax.rem(y + n_y - i, n_y) * 2 + core
            landed(source_at(n), from_block, fr.at[k], fs.at[k])
            here = xs.at[rows_of(source_at(n)), cols(from_block)]
            q = i * n_sp + n
            go(remote(here, here, qs.at[q], qr.at[q], partner))
    for n in range(n_sp):
        for i in range(n_y):
            from_block = lax.rem(y + n_y - i, n_y) * 2 + 1 - core
            q = i * n_sp + n
            landed(source_at(n), from_block, qr.at[q], qs.at[q])
    for copy in waits:
        copy.wait_send()


def dispatch_call(rows, w, skip, gain, hot):
    n_sp, n_tp = lax.axis_size("sp"), lax.axis_size("tp")
    n_y = n_tp // 2
    bf16, f32 = jnp.bfloat16, jnp.float32
    tok, width = skip.shape
    d_local = width // n_tp
    slots = hot.shape[0]
    cap = slots // n_sp
    more = max(n_y - 1, 1)
    return pl.pallas_call(
        dispatch_kernel,
        out_shape=(
            jax.ShapeDtypeStruct((tok, d_local), bf16),
            jax.ShapeDtypeStruct((slots, width), bf16),
        ),
        in_specs=[VM] * 5,
        out_specs=(VM, VM),
        scratch_shapes=[
            pltpu.VMEM((n_y, tok, d_local), bf16),
            pltpu.VMEM((n_y, tok, d_local), bf16),
            pltpu.VMEM((more, tok, d_local), bf16),
            pltpu.VMEM((more, tok, d_local), bf16),
            pltpu.VMEM((8, tok), f32),
            pltpu.VMEM((n_tp - 1, 8, tok), f32),
            pltpu.VMEM((n_sp - 1, cap, d_local), bf16),
            DMA((n_y,)),
            DMA((n_y,)),
            DMA((more,)),
            DMA((more,)),
            DMA((n_tp - 1,)),
            DMA((n_tp - 1,)),
            DMA((n_sp - 1,)),
            DMA((n_sp - 1,)),
            DMA((more * n_sp,)),
            DMA((more * n_sp,)),
            DMA((n_y * n_sp,)),
            DMA((n_y * n_sp,)),
        ],
        compiler_params=pltpu.CompilerParams(
            collective_id=1, has_side_effects=True, vmem_limit_bytes=VMEM_ROOM
        ),
        name="dispatch",
    )(rows, w, skip, gain, hot)


def return_kernel(
    down, stream, share, pick,
    out,
    precv, ysend, yrecv, rsend, ret,
    ps, pr, ys, yr, rs, rr,
):
    f32, bf16 = jnp.float32, jnp.bfloat16
    n_sp, n_tp, me, lane = places()
    n_y = n_tp // 2
    y, core = lane // 2, lax.rem(lane, 2)
    partner = (me, y * 2 + 1 - core)
    d_local = out.shape[1]
    cap = down.shape[0] // n_sp
    greet(
        [partner]
        + [(me, lax.rem(y + i, n_y) * 2 + core) for i in range(1, n_y)]
        + sp_peers(n_sp, me, lane)
    )

    def cols(block):
        return pl.ds(pl.multiple_of(block * d_local, 128), d_local)

    def rows_of(source):
        return pl.ds(pl.multiple_of(source * cap, 16), cap)

    def y_at(i):
        return lax.rem(y + i, n_y)

    def to_at(n):
        return lax.rem(me + n + 1, n_sp)

    waits = []

    def go(copy):
        copy.start()
        waits.append(copy)
        return copy

    pair, across, back = {}, {}, []
    for n in range(n_sp):
        for i in list(range(1, n_y)) + [0]:
            k = n * n_y + i
            src = down.at[rows_of(to_at(n)), cols(y_at(i) * 2 + 1 - core)]
            pair[n, i] = go(remote(src, precv.at[k], ps.at[k], pr.at[k], partner))
    for n in range(n_sp):
        for i in range(1, n_y):
            pair[n, i].wait_recv()
            k = n * (n_y - 1) + i - 1
            mine = down[rows_of(to_at(n)), cols(y_at(i) * 2 + core)].astype(f32)
            ysend[k] = (mine + precv[n * n_y + i].astype(f32)).astype(bf16)
            across[n, i] = go(
                remote(
                    ysend.at[k], yrecv.at[k], ys.at[k], yr.at[k], (me, y_at(i) * 2 + core)
                )
            )
    for n in range(n_sp):
        total = down[rows_of(to_at(n)), cols(lane)].astype(f32)
        pair[n, 0].wait_recv()
        total = total + precv[n * n_y].astype(f32)
        for i in range(1, n_y):
            across[n, i].wait_recv()
            total = total + yrecv[n * (n_y - 1) + i - 1].astype(f32)
        if n < n_sp - 1:
            rsend[n] = total.astype(bf16)
            back.append(
                go(remote(rsend.at[n], ret.at[rows_of(me), :], rs.at[n], rr.at[n], (to_at(n), lane)))
            )
        else:
            ret[rows_of(me), :] = total.astype(bf16)
    for n in range(n_sp - 1):
        here = ret.at[rows_of(lax.rem(me + n_sp - n - 1, n_sp)), :]
        remote(here, here, rs.at[n], rr.at[n], partner).wait_recv()
    combined = stream[...].astype(f32)
    rows_in = ret[...]
    moe = None
    for k in range(pick.shape[0]):
        chosen = jnp.dot(pick[k], rows_in, preferred_element_type=f32) * share[:, k : k + 1]
        moe = chosen if moe is None else moe + chosen
    out[...] = (combined + moe).astype(bf16)
    for copy in waits:
        copy.wait_send()


def return_call(down, stream, share, pick):
    n_sp, n_tp = lax.axis_size("sp"), lax.axis_size("tp")
    n_y = n_tp // 2
    bf16 = jnp.bfloat16
    tok, d_local = stream.shape
    slots = down.shape[0]
    cap = slots // n_sp
    more = max((n_y - 1) * n_sp, 1)
    return pl.pallas_call(
        return_kernel,
        out_shape=jax.ShapeDtypeStruct((tok, d_local), bf16),
        in_specs=[VM] * 4,
        out_specs=VM,
        scratch_shapes=[
            pltpu.VMEM((n_y * n_sp, cap, d_local), bf16),
            pltpu.VMEM((more, cap, d_local), bf16),
            pltpu.VMEM((more, cap, d_local), bf16),
            pltpu.VMEM((n_sp - 1, cap, d_local), bf16),
            pltpu.VMEM((slots, d_local), bf16),
            DMA((n_y * n_sp,)),
            DMA((n_y * n_sp,)),
            DMA((more,)),
            DMA((more,)),
            DMA((n_sp - 1,)),
            DMA((n_sp - 1,)),
        ],
        compiler_params=pltpu.CompilerParams(
            collective_id=2, has_side_effects=True, vmem_limit_bytes=VMEM_ROOM
        ),
        name="combine",
    )(down, stream, share, pick)


def affine_pair(earlier, latter):
    mul_re = earlier[0] * latter[0] - earlier[1] * latter[1]
    mul_im = earlier[0] * latter[1] + earlier[1] * latter[0]
    add_re = latter[0] * earlier[2] - latter[1] * earlier[3] + latter[2]
    add_im = latter[0] * earlier[3] + latter[1] * earlier[2] + latter[3]
    return (mul_re, mul_im, add_re, add_im)


def local_prefix(elements):
    length = elements[0].shape[2]
    fills = (1.0, 0.0, 0.0, 0.0)
    offset = 1
    while offset < length:
        earlier = tuple(
            (
                jnp.pad(
                    item[:, :, : length - offset],
                    ((0, 0), (0, 0), (offset, 0)),
                    constant_values=fill,
                )
                for item, fill in zip(elements, fills)
            )
        )
        elements = affine_pair(earlier, elements)
        offset = offset * 2
    return elements


def per_device(
    lane_source_signal,
    spectral_damping_part,
    spectral_angular_part,
    interval_exponent,
    entry_matrix_inphase,
    entry_matrix_quadrature,
    emission_inphase,
    emission_quadrature,
    lane_bypass_factor,
    spike_shrink_offset,
    lane_exit_matrix,
    skipline_stream,
    specialist_scaling_vector,
    selected_specialists,
    dispatcher_scores,
    specialist_valve_matrix,
    specialist_widen_matrix,
    specialist_shrink_matrix,
):
    f32 = jnp.float32
    bf16 = jnp.bfloat16
    groups_here = spectral_damping_part.shape[0]
    lanes_within_bundle = entry_matrix_inphase.shape[2]
    tok_local = lane_source_signal.shape[1]
    bundled_signal = lane_source_signal.astype(f32).reshape(
        groups_here, lanes_within_bundle, tok_local
    )
    step_size = jnp.exp(interval_exponent)[:, None]
    natural_pace_exponent = spectral_damping_part * step_size
    angle = spectral_angular_part * step_size
    num_re = jnp.expm1(natural_pace_exponent) * jnp.cos(angle) - 2.0 * jnp.sin(0.5 * angle) ** 2
    num_im = jnp.exp(natural_pace_exponent) * jnp.sin(angle)
    denom = (
        spectral_damping_part * spectral_damping_part
        + spectral_angular_part * spectral_angular_part
    )
    fac_re = (num_re * spectral_damping_part + num_im * spectral_angular_part) / denom
    fac_im = (num_im * spectral_damping_part - num_re * spectral_angular_part) / denom
    map_re = (
        fac_re[:, :, None] * entry_matrix_inphase - fac_im[:, :, None] * entry_matrix_quadrature
    )
    map_im = (
        fac_re[:, :, None] * entry_matrix_quadrature + fac_im[:, :, None] * entry_matrix_inphase
    )
    drive_re = jnp.einsum("gpc,gct->gpt", map_re, bundled_signal, precision=PRECISE_MODE)
    drive_im = jnp.einsum("gpc,gct->gpt", map_im, bundled_signal, precision=PRECISE_MODE)
    recurrence_modulus = jnp.exp(
        natural_pace_exponent[:, :, None] + spike_shrink_offset[:, None, :]
    )
    trans_re = recurrence_modulus * jnp.cos(angle)[:, :, None]
    trans_im = recurrence_modulus * jnp.sin(angle)[:, :, None]
    cum_re, cum_im, state_real, state_imaginary = local_prefix(
        (trans_re, trans_im, drive_re, drive_im)
    )
    summary = jnp.stack(
        [
            plane[:, :, -1].reshape(-1, 128)
            for plane in (cum_re, cum_im, state_real, state_imaginary)
        ]
    )
    entering = carry_call(summary)
    enter_re = entering[0].reshape(groups_here, -1)[:, :, None]
    enter_im = entering[1].reshape(groups_here, -1)[:, :, None]
    state_real = state_real + cum_re * enter_re - cum_im * enter_im
    state_imaginary = state_imaginary + cum_re * enter_im + cum_im * enter_re
    value = (
        jnp.einsum("nef,nfi->nei", emission_inphase, state_real, precision=PRECISE_MODE)
        - jnp.einsum("nef,nfi->nei", emission_quadrature, state_imaginary, precision=PRECISE_MODE)
        + lane_bypass_factor.reshape(groups_here, lanes_within_bundle)[:, :, None] * bundled_signal
    )
    recurrence_result = (
        jax.nn.gelu(value).astype(bf16).reshape(groups_here * lanes_within_bundle, tok_local)
    )
    share = dispatcher_scores / jnp.sum(dispatcher_scores, axis=1, keepdims=True)
    experts = lax.axis_size("sp")
    top = selected_specialists.shape[1]
    capacity = 2 * tok_local * top // experts
    flat_routes = selected_specialists.reshape(-1)
    hits = (flat_routes[:, None] == jnp.arange(experts, dtype=jnp.int32)[None, :]).astype(jnp.int32)
    ranks = jnp.sum((jnp.cumsum(hits, axis=0) - hits) * hits, axis=1)
    slot_ids = (flat_routes * capacity + ranks).reshape(tok_local, top)
    slot_grid = jnp.arange(experts * capacity, dtype=jnp.int32)
    pick = jnp.stack(
        [(slot_ids[:, k : k + 1] == slot_grid[None, :]).astype(bf16) for k in range(top)]
    )
    hot = jnp.any(slot_grid[:, None, None] == slot_ids.T[None, :, :], axis=1).astype(bf16)
    stream, rows = dispatch_call(
        recurrence_result.T,
        lane_exit_matrix,
        skipline_stream,
        specialist_scaling_vector[None, :],
        hot,
    )
    gate_part = jnp.dot(rows, specialist_valve_matrix[0], preferred_element_type=f32)
    up_part = jnp.dot(rows, specialist_widen_matrix[0], preferred_element_type=f32)
    hidden = (jax.nn.silu(gate_part) * up_part).astype(bf16)
    down_part = jnp.dot(hidden, specialist_shrink_matrix[0], preferred_element_type=f32).astype(bf16)
    return return_call(down_part, stream, share, pick)


def solution(mesh):
    placed = (
        P("tp", "sp"),
        P("tp", None),
        P("tp", None),
        P("tp"),
        P("tp", None, None),
        P("tp", None, None),
        P("tp", None, None),
        P("tp", None, None),
        P("tp"),
        P("tp", "sp"),
        P("tp", None),
        P("sp", None),
        P(),
        P("sp", None),
        P("sp", None),
        P("sp", None, "tp"),
        P("sp", None, "tp"),
        P("sp", "tp", None),
    )
    return jax.shard_map(
        per_device, mesh=mesh, in_specs=placed, out_specs=P("sp", "tp"), check_vma=False
    )
```

time: 371 us -> 144 us (0.39); the launches traced: 366 us -> 143 us
  waiting for transfers between devices: 167 us -> 0 us
  blocking collectives: 122 us -> 0 us
  Pallas kernels: 0 us -> 106 us
  between operations: 13.5 us -> 0.29 us
  local copies, waits for them, and re-layouts: 19.4 us -> 6.7 us
  starting transfers between devices: 5.75 us -> 0 us
  other arithmetic: 17.3 us -> 12.6 us
    pallas_call x0 -> x3, Pallas kernels: none -> 106 us  [the longest x1 52.5 us: dispatch_call(): pl.pallas_call(dispatch_kernel, out_shape=(jax.ShapeDtypeStruct((tok, d_l...]
    all_gather x4 -> x0, blocking collectives: 94.3 us -> none  [carried_in(): pieces = jax.tree.map(lambda part: lax.all_gather(part, axis), value)]
    psum x1 -> x0, waiting for transfers between devices: 62.8 us -> none  [per_device(): lax.psum(partial_rows.astype(jnp.bfloat16), 'tp').astype(jnp.float32)]
    reduce_scatter x1 -> x0, waiting for transfers between devices: 44 us -> none  [per_device(): lax.psum_scatter(down_part.astype(f32).astype(jnp.bfloat16), 'tp', scatte...]
    all_gather x1 -> x0, waiting for transfers between devices: 37.3 us -> none  [per_device(): piece = lax.all_gather(arrived, 'tp', axis=2, tiled=True)]
    all_to_all x1 -> x0, blocking collectives: 27.8 us -> none  [per_device(): lax.all_to_all(dispatch, 'sp', split_axis=0, concat_axis=0, tiled=True)]
    all_to_all x1 -> x0, waiting for transfers between devices: 22.8 us -> none  [per_device(): lax.all_to_all(expert_out, 'sp', split_axis=0, concat_axis=0, tiled=True)]
    slice x9 -> x5, local copies, waits for them, and re-layouts: 11.3 us -> 2.32 us  [the longest x3 1.42 us: per_device(): plane[:, :, -1].reshape(-1, 128)]
  transfers between devices with their start and end apart: 4 -> 0, of which waited for: 4 -> 0; matrix products, arithmetic and copies ran while one was open for 1% -> 0% of each run, Pallas kernels for 0% -> 0%
where the time goes in v1:
time: 144 us; the launch traced here: 143 us
  Pallas kernels  106 us (74%)
  matrix products  17.5 us (12%)
  other arithmetic  12.6 us (9%)
  local copies, waits for them, and re-layouts  6.7 us (5%)
    pallas_call x1, Pallas kernels, dispatch_call(): pl.pallas_call(dispatch_kernel, out_shape=(jax.ShapeDtypeStruct((tok, d_l...  52.5 us
    pallas_call x1, Pallas kernels, return_call(): pl.pallas_call(return_kernel, out_shape=jax.ShapeDtypeStruct((tok, d_loca...  45.3 us
    pallas_call x1, Pallas kernels, carry_call(): pl.pallas_call(carry_kernel, out_shape=jax.ShapeDtypeStruct((2,) + summar...  8.58 us
    dot_general x1, matrix products, per_device(): jnp.dot(rows, specialist_valve_matrix[0], preferred_element_type=f32)  5.92 us
    dot_general x1, matrix products, per_device(): jnp.dot(hidden, specialist_shrink_matrix[0], preferred_element_type=f32)  4.34 us
    add x6, other arithmetic, affine_pair(): add_im = latter[0] * earlier[3] + latter[1] * earlier[2] + latter[3]  4.09 us
    add x6, other arithmetic, affine_pair(): add_re = latter[0] * earlier[2] - latter[1] * earlier[3] + latter[2]  3.17 us

profile of v1, /device:TPU:11, one launch (start us, length us, event | category | flops | bytes accessed | tf_op | source)
XLA Modules:
  0.0 143.5 jit_solution(17238075141127826924)
XLA Ops:
  0.0 0.7 exp.13
  0.7 0.9 fusion.55
  1.6 1.6 %fusion.41 = f32[16,64,128]{2,1,0:T(8,128)S(1)} fusion(bf16[16,16,128]{2,1,0:T(8,128)(2,1)} %bitcast.113, f32[16,64,16]{1,2,0:T(8,128)} %param.22, f32[16,64,16]{1,2,0:T(8,128)} %param.23, f32[16,64]{1,0:T(8,128)S(1)} %get-tuple-element.35, f32[16,64]{1,0:T(8,128)S(1)} %get-tuple-element.34), kind=kOutput, calls=%fused_computation.73 | convolution fusion | flops 25214976 | bytes 729088 | tf_op jit(solution)/shard_map/gpc,gct->gpt/dot_general | solution.py:457
  3.2 1.6 %fusion.45 = f32[16,64,128]{2,1,0:T(8,128)S(1)} fusion(bf16[16,16,128]{2,1,0:T(8,128)(2,1)} %bitcast.114, f32[16,64,16]{1,2,0:T(8,128)} %param.23, f32[16,64,16]{1,2,0:T(8,128)} %param.22, f32[16,64]{1,0:T(8,128)S(1)} %get-tuple-element.35, f32[16,64]{1,0:T(8,128)S(1)} %get-tuple-element.34), kind=kOutput, calls=%fused_computation.77 | convolution fusion | flops 25214976 | bytes 729088 | tf_op jit(solution)/shard_map/gpc,gct->gpt/dot_general | solution.py:456
  4.8 1.5 %subtract_add_fusion.6 = (f32[16,64,128]{2,1,0:T(8,128)S(1)}, f32[16,64,128]{2,1,0:T(8,128)S(1)}, f32[16,64,128]{2,1,0:T(8,128)S(1)}, f32[16,64,128]{2,1,0:T(8,128)S(1)}) fusion(f32[16,64,128]{2,1,0:T(8,128)S(1)} %fusion.45, f32[16,64,127]{2,1,0:T(8,128)S(1)} %bitcast.109, f32[16,64,127]{2,1,0:T(8,128)S(1)} %bitcast.110, f32[16,64]{1,0:T(8,128)S(1)} %get-tuple-element.38, ...), kind=kLoop, calls=%fused_computation.41 | loop fusion | flops 1441792 | bytes 4206592 | tf_op jit(solution)/shard_map/add | solution.py:386
  6.2 1.0 add_add_fusion.5
  7.6 0.6 add_add_fusion.4
  8.6 0.6 add_add_fusion.3
  12.7 0.6 slice_reduce_fusion.1
  15.1 8.6 %carry.1 = f32[2,8,128]{2,1,0:T(8,128)} custom-call(f32[4,8,128]{2,1,0:T(8,128)} %pad_maximum_fusion.mine), custom_call_target="tpu_custom_call" | custom-call | tf_op jit(solution)/shard_map/carry/pallas_call | solution.py:64
  23.7 0.7 fusion.57
  24.5 0.8 fusion.17
  25.4 0.8 fusion.38
  26.2 0.7 copy.42
  27.2 0.8 reduce-window.6
  28.8 0.7 convert_element_type.39.hot
  29.5 52.5 %dispatch.1 = (bf16[128,1024]{1,0:T(8,128)(2,1)}, bf16[512,4096]{1,0:T(8,128)(2,1)}) custom-call(bf16[128,256]{1,0:T(8,128)(2,1)} %bitcast.116, bf16[256,4096]{1,0:T(8,128)(2,1)} %w.1, bf16[128,4096]{1,0:T(8,128)(2,1)} %skip.1, f32[1,4096]{1,0:T(1,128)} %bitcast.118, bf16[512,128]{1,0:T(8,128)(2,1)} %convert_element_type.39.hot), custom_call_target="tpu_custom_call" | custom-call | tf_op jit(solution)/shard_map/dispatch/pallas_call | solution.py:231
  82.1 5.9 %fusion.3 = f32[512,512]{1,0:T(8,128)S(1)} fusion(bf16[512,4096]{1,0:T(8,128)(2,1)} %get-tuple-element.7, bf16[1,4096,512]{2,1,0:T(8,128)(2,1)} %param.33), kind=kOutput, calls=%fused_computation.4 | convolution fusion | flops 2147483648 | bytes 9437184 | tf_op jit(solution)/shard_map/dot_general | solution.py:505
  88.0 2.4 %fusion.8 = bf16[512,512]{1,0:T(8,128)(2,1)S(1)} fusion(bf16[512,4096]{1,0:T(8,128)(2,1)S(1)} %copy-done.9, bf16[1,4096,512]{2,1,0:T(8,128)(2,1)S(1)} %copy-done.7, f32[512,512]{1,0:T(8,128)S(1)} %fusion.3), kind=kOutput, calls=%fused_computation.7 | convolution fusion | flops 2149056512 | bytes 9961472 | tf_op jit(solution)/shard_map/dot_general | solution.py:506
  90.5 4.3 %convolution_convert_fusion.down = bf16[512,4096]{1,0:T(8,128)(2,1)} fusion(bf16[512,512]{1,0:T(8,128)(2,1)S(1)} %fusion.8, bf16[1,512,4096]{2,1,0:T(8,128)(2,1)S(1)} %copy-done.8), kind=kOutput, calls=%fused_computation | convolution fusion | flops 2149580800 | bytes 8912896 | tf_op jit(solution)/shard_map/dot_general | solution.py:508
  95.0 0.7 add_convert_fusion.pick
  95.8 0.7 broadcast_divide_fusion.share
  96.5 45.3 %combine.1 = bf16[128,1024]{1,0:T(8,128)(2,1)} custom-call(bf16[512,4096]{1,0:T(8,128)(2,1)} %convolution_convert_fusion.down, bf16[128,1024]{1,0:T(8,128)(2,1)} %get-tuple-element.8.stream, f32[128,2]{1,0:T(8,128)} %broadcast_divide_fusion.share, bf16[2,128,512]{2,1,0:T(8,128)(2,1)} %add_convert_fusion.pick), custom_call_target="tpu_custom_call" | custom-call | tf_op jit(solution)/shard_map/combine/pallas_call | solution.py:358
  141.8 1.7 %copy.49 = bf16[128,1024]{1,0:T(8,128)(2,1)} copy(bf16[128,1024]{1,0:T(8,128)(2,1)} %combine.1) | data formatting | bytes 524288
  (55 shorter events, 7.4 us)
Async XLA Ops:
  0.0 24.5 %copy-start = (f32[16,16,64]{2,1,0:T(8,128)S(1)}, f32[16,16,64]{2,1,0:T(8,128)}, u32[]{:S(2)}) copy-start(f32[16,16,64]{2,1,0:T(8,128)} %param.24) | copy-start | bytes 196612
  0.0 6.2 %copy-start.3 = (f32[16,128]{1,0:T(8,128)S(1)}, f32[16,128]{1,0:T(8,128)}, u32[]{:S(2)}) copy-start(f32[16,128]{1,0:T(8,128)} %param.27) | copy-start | bytes 24580
  12.1 13.2 %copy-start.6 = (f32[256]{0:T(256)S(1)}, f32[256]{0:T(256)}, u32[]{:S(2)}) copy-start(f32[256]{0:T(256)} %param.26) | copy-start | bytes 3076
  12.1 13.3 %copy-start.1 = (bf16[256,128]{1,0:T(8,128)(2,1)S(1)}, bf16[256,128]{1,0:T(8,128)(2,1)}, u32[]{:S(2)}) copy-start(bf16[256,128]{1,0:T(8,128)(2,1)} %param.18) | copy-start | bytes 196612
  12.1 13.3 %copy-start.2 = (f32[16,16,64]{2,1,0:T(8,128)S(1)}, f32[16,16,64]{2,1,0:T(8,128)}, u32[]{:S(2)}) copy-start(f32[16,16,64]{2,1,0:T(8,128)} %param.25) | copy-start | bytes 196612
  12.7 14.2 %copy-start.4 = (s32[128,2]{0,1:T(2,128)S(1)}, s32[128,2]{0,1:T(2,128)}, u32[]{:S(2)}) copy-start(s32[128,2]{0,1:T(2,128)} %param.31) | copy-start | bytes 3076
  82.0 6.0 %copy-start.7 = (bf16[1,4096,512]{2,1,0:T(8,128)(2,1)S(1)}, bf16[1,4096,512]{2,1,0:T(8,128)(2,1)}, u32[]{:S(2)}) copy-start(bf16[1,4096,512]{2,1,0:T(8,128)(2,1)} %param.34) | copy-start | bytes 12582916
  82.0 5.9 %copy-start.9 = (bf16[512,4096]{1,0:T(8,128)(2,1)S(1)}, bf16[512,4096]{1,0:T(8,128)(2,1)}, u32[]{:S(2)}) copy-start(bf16[512,4096]{1,0:T(8,128)(2,1)} %get-tuple-element.7) | copy-start | bytes 12582916
  88.0 2.5 %copy-start.8 = (bf16[1,512,4096]{2,1,0:T(8,128)(2,1)S(1)}, bf16[1,512,4096]{2,1,0:T(8,128)(2,1)}, u32[]{:S(2)}) copy-start(bf16[1,512,4096]{2,1,0:T(8,128)(2,1)} %param.35) | copy-start | bytes 12582916
  90.5 5.2 %copy-start.5 = (f32[128,2]{0,1:T(2,128)S(1)}, f32[128,2]{0,1:T(2,128)}, u32[]{:S(2)}) copy-start(f32[128,2]{0,1:T(2,128)} %param.32) | copy-start | bytes 3076

commit v2 on v1

--- a/solution.py
+++ b/solution.py
@@ -12,7 +12,7 @@
 MESH = pl.DeviceIdType.MESH
 VM = pl.BlockSpec(memory_space=pltpu.VMEM)
 DMA = pltpu.SemaphoreType.DMA
-VMEM_ROOM = 60 * 1024 * 1024
+VMEM_ROOM = 48 * 1024 * 1024
 
 
 def greet(peers):
@@ -258,16 +258,16 @@
             DMA((n_y * n_sp,)),
         ],
         compiler_params=pltpu.CompilerParams(
-            collective_id=1, has_side_effects=True, vmem_limit_bytes=VMEM_ROOM
+            collective_id=1, has_side_effects=True, vmem_limit_bytes=VMEM_ROOM // 2
         ),
         name="dispatch",
     )(rows, w, skip, gain, hot)
 
 
 def return_kernel(
-    down, stream, share, pick,
+    hidden, w, share, pick,
     out,
-    precv, ysend, yrecv, rsend, ret,
+    psend, own, precv, ysend, yrecv, rsend, ret,
     ps, pr, ys, yr, rs, rr,
 ):
     f32, bf16 = jnp.float32, jnp.bfloat16
@@ -276,7 +276,7 @@
     y, core = lane // 2, lax.rem(lane, 2)
     partner = (me, y * 2 + 1 - core)
     d_local = out.shape[1]
-    cap = down.shape[0] // n_sp
+    cap = hidden.shape[0] // n_sp
     greet(
         [partner]
         + [(me, lax.rem(y + i, n_y) * 2 + core) for i in range(1, n_y)]
@@ -303,24 +303,31 @@
         return copy
 
     pair, across, back = {}, {}, []
+    def part(n, block):
+        return jnp.dot(hidden[rows_of(to_at(n)), :], w[:, cols(block)], preferred_element_type=f32)
+
+    order = list(range(1, n_y)) + [0]
+    for n in range(n_sp + 1):
+        if n < n_sp:
+            for i in order:
+                k = n * n_y + i
+                psend[k] = part(n, y_at(i) * 2 + 1 - core).astype(bf16)
+                pair[n, i] = go(remote(psend.at[k], precv.at[k], ps.at[k], pr.at[k], partner))
+            for i in order:
+                own[n * n_y + i] = part(n, y_at(i) * 2 + core)
+        if n > 0:
+            for i in range(1, n_y):
+                pair[n - 1, i].wait_recv()
+                j = (n - 1) * n_y + i
+                k = (n - 1) * (n_y - 1) + i - 1
+                ysend[k] = (own[j] + precv[j].astype(f32)).astype(bf16)
+                across[n - 1, i] = go(
+                    remote(
+                        ysend.at[k], yrecv.at[k], ys.at[k], yr.at[k], (me, y_at(i) * 2 + core)
+                    )
+                )
     for n in range(n_sp):
-        for i in list(range(1, n_y)) + [0]:
-            k = n * n_y + i
-            src = down.at[rows_of(to_at(n)), cols(y_at(i) * 2 + 1 - core)]
-            pair[n, i] = go(remote(src, precv.at[k], ps.at[k], pr.at[k], partner))
-    for n in range(n_sp):
-        for i in range(1, n_y):
-            pair[n, i].wait_recv()
-            k = n * (n_y - 1) + i - 1
-            mine = down[rows_of(to_at(n)), cols(y_at(i) * 2 + core)].astype(f32)
-            ysend[k] = (mine + precv[n * n_y + i].astype(f32)).astype(bf16)
-            across[n, i] = go(
-                remote(
-                    ysend.at[k], yrecv.at[k], ys.at[k], yr.at[k], (me, y_at(i) * 2 + core)
-                )
-            )
-    for n in range(n_sp):
-        total = down[rows_of(to_at(n)), cols(lane)].astype(f32)
+        total = own[n * n_y]
         pair[n, 0].wait_recv()
         total = total + precv[n * n_y].astype(f32)
         for i in range(1, n_y):
@@ -336,31 +343,32 @@
     for n in range(n_sp - 1):
         here = ret.at[rows_of(lax.rem(me + n_sp - n - 1, n_sp)), :]
         remote(here, here, rs.at[n], rr.at[n], partner).wait_recv()
-    combined = stream[...].astype(f32)
     rows_in = ret[...]
     moe = None
     for k in range(pick.shape[0]):
         chosen = jnp.dot(pick[k], rows_in, preferred_element_type=f32) * share[:, k : k + 1]
         moe = chosen if moe is None else moe + chosen
-    out[...] = (combined + moe).astype(bf16)
+    out[...] = moe
     for copy in waits:
         copy.wait_send()
 
 
-def return_call(down, stream, share, pick):
+def return_call(hidden, w, share, pick):
     n_sp, n_tp = lax.axis_size("sp"), lax.axis_size("tp")
     n_y = n_tp // 2
-    bf16 = jnp.bfloat16
-    tok, d_local = stream.shape
-    slots = down.shape[0]
+    bf16, f32 = jnp.bfloat16, jnp.float32
+    tok, d_local = share.shape[0], w.shape[1] // n_tp
+    slots = hidden.shape[0]
     cap = slots // n_sp
     more = max((n_y - 1) * n_sp, 1)
     return pl.pallas_call(
         return_kernel,
-        out_shape=jax.ShapeDtypeStruct((tok, d_local), bf16),
+        out_shape=jax.ShapeDtypeStruct((tok, d_local), f32),
         in_specs=[VM] * 4,
         out_specs=VM,
         scratch_shapes=[
+            pltpu.VMEM((n_y * n_sp, cap, d_local), bf16),
+            pltpu.VMEM((n_y * n_sp, cap, d_local), f32),
             pltpu.VMEM((n_y * n_sp, cap, d_local), bf16),
             pltpu.VMEM((more, cap, d_local), bf16),
             pltpu.VMEM((more, cap, d_local), bf16),
@@ -377,7 +385,7 @@
             collective_id=2, has_side_effects=True, vmem_limit_bytes=VMEM_ROOM
         ),
         name="combine",
-    )(down, stream, share, pick)
+    )(hidden, w, share, pick)
 
 
 def affine_pair(earlier, latter):
@@ -505,8 +513,8 @@
     gate_part = jnp.dot(rows, specialist_valve_matrix[0], preferred_element_type=f32)
     up_part = jnp.dot(rows, specialist_widen_matrix[0], preferred_element_type=f32)
     hidden = (jax.nn.silu(gate_part) * up_part).astype(bf16)
-    down_part = jnp.dot(hidden, specialist_shrink_matrix[0], preferred_element_type=f32).astype(bf16)
-    return return_call(down_part, stream, share, pick)
+    moe = return_call(hidden, specialist_shrink_matrix[0], share, pick)
+    return (stream.astype(f32) + moe).astype(bf16)
 
 
 def solution(mesh):

time: 144 us -> 141 us (0.979)
  Pallas kernels: 106 us -> 100 us
  local copies, waits for them, and re-layouts: 6.7 us -> 10.7 us
  matrix products: 17.5 us -> 14.7 us
    dot_general x1 -> x0, matrix products: 4.34 us -> none  [per_device(): jnp.dot(hidden, specialist_shrink_matrix[0], preferred_element_type=f32)]
    pallas_call x1, Pallas kernels: 52.5 us -> 48.8 us  [dispatch_call(): pl.pallas_call(dispatch_kernel, out_shape=(jax.ShapeDtypeStruct((tok, d_l...]
    pallas_call x1, Pallas kernels: 45.3 us -> 43.1 us  [return_call(): pl.pallas_call(return_kernel, out_shape=jax.ShapeDtypeStruct((tok, d_loca...]
    slice x3, local copies, waits for them, and re-layouts: 1.42 us -> 3.5 us  [per_device(): plane[:, :, -1].reshape(-1, 128)]
    unnamed x23 -> x34, local copies, waits for them, and re-layouts: 1.95 us -> 3.94 us
where the time goes in v2:
time: 141 us; the launch traced here: 140 us
  Pallas kernels  100 us (71%)
  matrix products  14.7 us (10%)
  other arithmetic  13.9 us (10%)
  local copies, waits for them, and re-layouts  10.7 us (8%)
    pallas_call x1, Pallas kernels, dispatch_call(): pl.pallas_call(dispatch_kernel, out_shape=(jax.ShapeDtypeStruct((tok, d_l...  48.8 us
    pallas_call x1, Pallas kernels, return_call(): pl.pallas_call(return_kernel, out_shape=jax.ShapeDtypeStruct((tok, d_loca...  43.1 us
    pallas_call x1, Pallas kernels, carry_call(): pl.pallas_call(carry_kernel, out_shape=jax.ShapeDtypeStruct((2,) + summar...  8.58 us
    add x6, other arithmetic, affine_pair(): add_im = latter[0] * earlier[3] + latter[1] * earlier[2] + latter[3]  4.89 us
    dot_general x1, matrix products, per_device(): jnp.dot(rows, specialist_valve_matrix[0], preferred_element_type=f32)  4.66 us
    unnamed x34, local copies, waits for them, and re-layouts  3.94 us
    slice x3, local copies, waits for them, and re-layouts, per_device(): plane[:, :, -1].reshape(-1, 128)  3.5 us
    add x6, other arithmetic, affine_pair(): add_re = latter[0] * earlier[2] - latter[1] * earlier[3] + latter[2]  3.41 us

profile of v2, /device:TPU:11, one launch (start us, length us, event | category | flops | bytes accessed | tf_op | source)
XLA Modules:
  0.0 140.1 jit_solution(9612411070828648498)
XLA Ops:
  0.0 0.7 exp.13
  0.7 0.9 fusion.54
  1.6 1.6 %fusion.40 = f32[16,64,128]{2,1,0:T(8,128)S(1)} fusion(bf16[16,16,128]{2,1,0:T(8,128)(2,1)} %bitcast.113, f32[16,64,16]{1,2,0:T(8,128)} %param.22, f32[16,64,16]{1,2,0:T(8,128)} %param.23, f32[16,64]{1,0:T(8,128)S(1)} %get-tuple-element.35, f32[16,64]{1,0:T(8,128)S(1)} %get-tuple-element.34), kind=kOutput, calls=%fused_computation.72 | convolution fusion | flops 25214976 | bytes 729088 | tf_op jit(solution)/shard_map/gpc,gct->gpt/dot_general | solution.py:465
  3.2 1.6 %fusion.44 = f32[16,64,128]{2,1,0:T(8,128)S(1)} fusion(bf16[16,16,128]{2,1,0:T(8,128)(2,1)} %bitcast.114, f32[16,64,16]{1,2,0:T(8,128)} %param.23, f32[16,64,16]{1,2,0:T(8,128)} %param.22, f32[16,64]{1,0:T(8,128)S(1)} %get-tuple-element.35, f32[16,64]{1,0:T(8,128)S(1)} %get-tuple-element.34), kind=kOutput, calls=%fused_computation.76 | convolution fusion | flops 25214976 | bytes 729088 | tf_op jit(solution)/shard_map/gpc,gct->gpt/dot_general | solution.py:464
  4.8 1.5 %subtract_add_fusion.6 = (f32[16,64,128]{2,1,0:T(8,128)S(1)}, f32[16,64,128]{2,1,0:T(8,128)S(1)}, f32[16,64,128]{2,1,0:T(8,128)S(1)}, f32[16,64,128]{2,1,0:T(8,128)S(1)}) fusion(f32[16,64,128]{2,1,0:T(8,128)S(1)} %fusion.44, f32[16,64,127]{2,1,0:T(8,128)S(1)} %bitcast.109, f32[16,64,127]{2,1,0:T(8,128)S(1)} %bitcast.110, f32[16,64]{1,0:T(8,128)S(1)} %get-tuple-element.38, ...), kind=kLoop, calls=%fused_computation.40 | loop fusion | flops 1441792 | bytes 4206592 | tf_op jit(solution)/shard_map/add | solution.py:394
  6.2 1.0 add_add_fusion.5
  11.7 1.4 add_add_fusion
  13.1 1.4 %multiply_subtract_fusion = (f32[16,64,128]{2,1,0:T(8,128)}, f32[16,64,128]{2,1,0:T(8,128)S(1)}, f32[16,64,128]{2,1,0:T(8,128)S(1)}) fusion(f32[16,64,128]{2,1,0:T(8,128)S(1)} %get-tuple-element.10, f32[16,64,128]{2,1,0:T(8,128)S(1)} %get-tuple-element.11, f32[16,64,64]{2,1,0:T(8,128)S(1)} %bitcast.107, f32[16,64,64]{2,1,0:T(8,128)S(1)} %bitcast.108, ...), kind=kLoop, calls=%fused_computation.26 | loop fusion | flops 1310720 | bytes 4194304 | tf_op jit(solution)/shard_map/sub | solution.py:392
  14.6 0.8 copy-done.7
  16.1 1.4 %slice_reduce_fusion.3 = f32[16,64]{1,0:T(8,128)S(1)} fusion(f32[16,64,128]{2,1,0:T(8,128)} %get-tuple-element.27), kind=kLoop, calls=%fused_computation.12 | loop fusion | bytes 8192 | tf_op jit(solution)/shard_map/slice | solution.py:476
  17.7 1.4 %slice_reduce_fusion = f32[16,64]{1,0:T(8,128)S(1)} fusion(f32[16,64,128]{2,1,0:T(8,128)} %get-tuple-element.9), kind=kLoop, calls=%fused_computation.9 | loop fusion | bytes 8192 | tf_op jit(solution)/shard_map/slice | solution.py:476
  19.8 8.6 %carry.1 = f32[2,8,128]{2,1,0:T(8,128)} custom-call(f32[4,8,128]{2,1,0:T(8,128)} %pad_maximum_fusion.mine), custom_call_target="tpu_custom_call" | custom-call | tf_op jit(solution)/shard_map/carry/pallas_call | solution.py:64
  28.4 0.7 fusion.56
  29.2 2.2 %fusion.16 = f32[16,128,16]{1,2,0:T(8,128)S(1)} fusion(f32[16,16,64]{2,1,0:T(8,128)S(1)} %copy-done, f32[16,64,128]{2,1,0:T(8,128)} %copy-done.7, f32[16,64,128]{2,1,0:T(8,128)} %copy-done.8, f32[16,64,128]{2,1,0:T(8,128)} %get-tuple-element.27, f32[16,64]{1,0:T(8,128)S(1)} %mul.426, f32[16,64]{1,0:T(8,128)S(1)} %mul.423), kind=kOutput, calls=%fused_computation.19 | convolution fusion | flops 25690112 | bytes 1777664 | tf_op jit(solution)/shard_map/nef,nfi->nei/dot_general | solution.py:486
  32.1 2.2 %fusion.37 = bf16[16,16,128]{2,1,0:T(8,128)(2,1)S(1)} fusion(f32[16,128,16]{1,2,0:T(8,128)S(1)} %fusion.16, f32[16,16,64]{2,1,0:T(8,128)} %param.25, f32[16,64,128]{2,1,0:T(8,128)} %copy-done.7, f32[16,64,128]{2,1,0:T(8,128)} %get-tuple-element.9, f32[16,64,128]{2,1,0:T(8,128)} %get-tuple-element.27, f32[16,64]{1,0:T(8,128)} %copy-done.11, ...), kind=kOutput, calls=%fused_computation.71 | convolution fusion | flops 26116096 | bytes 1909760 | tf_op jit(solution)/shard_map/nef,nfi->nei/dot_general | solution.py:487
  34.4 0.8 copy.43
  35.4 0.8 reduce-window.6
  36.8 0.7 multiply_add_fusion.8
  37.7 48.8 %dispatch.1 = (bf16[128,1024]{1,0:T(8,128)(2,1)S(1)}, bf16[512,4096]{1,0:T(8,128)(2,1)S(1)}) custom-call(bf16[128,256]{1,0:T(8,128)(2,1)S(1)} %bitcast.71, bf16[256,4096]{1,0:T(8,128)(2,1)S(1)} %copy-done.2, bf16[128,4096]{1,0:T(8,128)(2,1)S(1)} %copy-done.3, f32[1,4096]{1,0:T(1,128)S(1)} %bitcast.72, bf16[512,128]{1,0:T(8,128)(2,1)S(1)} %convert_element_type.42.hot), custom_call_target="tpu_custom_call" | custom-call | tf_op jit(solution)/shard_map/dispatch/pallas_call | solution.py:231
  86.5 4.7 %fusion.2 = f32[512,512]{1,0:T(8,128)S(1)} fusion(bf16[512,4096]{1,0:T(8,128)(2,1)S(1)} %get-tuple-element.8, bf16[1,4096,512]{2,1,0:T(8,128)(2,1)} %param.33), kind=kOutput, calls=%fused_computation.2 | convolution fusion | flops 2147483648 | bytes 9437184 | tf_op jit(solution)/shard_map/dot_general | solution.py:513
  91.2 2.5 %fusion.7.hidden = bf16[512,512]{1,0:T(8,128)(2,1)S(1)} fusion(bf16[512,4096]{1,0:T(8,128)(2,1)S(1)} %get-tuple-element.8, bf16[1,4096,512]{2,1,0:T(8,128)(2,1)S(1)} %copy-done.15, f32[512,512]{1,0:T(8,128)S(1)} %fusion.2), kind=kOutput, calls=%fused_computation.5 | convolution fusion | flops 2149056512 | bytes 9961472 | tf_op jit(solution)/shard_map/dot_general | solution.py:514
  94.1 2.2 %copy-done.1 = bf16[1,512,4096]{2,1,0:T(8,128)(2,1)S(1)} copy-done((bf16[1,512,4096]{2,1,0:T(8,128)(2,1)S(1)}, bf16[1,512,4096]{2,1,0:T(8,128)(2,1)}, u32[]{:S(2)}) %copy-start.1) | copy-done | bytes 4194328
  96.2 43.1 %combine.1 = f32[128,1024]{1,0:T(8,128)S(1)} custom-call(bf16[512,512]{1,0:T(8,128)(2,1)S(1)} %fusion.7.hidden, bf16[512,4096]{1,0:T(8,128)(2,1)S(1)} %bitcast.70, f32[128,2]{1,0:T(8,128)S(1)} %broadcast_divide_fusion.share, bf16[2,128,512]{2,1,0:T(8,128)(2,1)S(1)} %add_convert_fusion.1.pick), custom_call_target="tpu_custom_call" | custom-call | tf_op jit(solution)/shard_map/combine/pallas_call | solution.py:364
  139.4 0.8 add_convert_fusion
  (66 shorter events, 8.2 us)
Async XLA Ops:
  0.0 29.2 %copy-start = (f32[16,16,64]{2,1,0:T(8,128)S(1)}, f32[16,16,64]{2,1,0:T(8,128)}, u32[]{:S(2)}) copy-start(f32[16,16,64]{2,1,0:T(8,128)} %param.24) | copy-start | bytes 196612
  0.0 6.2 %copy-start.12 = (f32[16,128]{1,0:T(8,128)S(1)}, f32[16,128]{1,0:T(8,128)}, u32[]{:S(2)}) copy-start(f32[16,128]{1,0:T(8,128)} %param.27) | copy-start | bytes 24580
  13.1 18.3 %copy-start.14 = (f32[256]{0:T(256)S(1)}, f32[256]{0:T(256)}, u32[]{:S(2)}) copy-start(f32[256]{0:T(256)} %param.26) | copy-start | bytes 3076
  13.1 19.0 %copy-start.9 = (bf16[256,128]{1,0:T(8,128)(2,1)S(1)}, bf16[256,128]{1,0:T(8,128)(2,1)}, u32[]{:S(2)}) copy-start(bf16[256,128]{1,0:T(8,128)(2,1)} %param.18) | copy-start | bytes 196612
  14.5 0.8 copy-start.7
  14.5 1.5 %copy-start.8 = (f32[16,64,128]{2,1,0:T(8,128)}, f32[16,64,128]{2,1,0:T(8,128)S(1)}, u32[]{:S(2)}) copy-start(f32[16,64,128]{2,1,0:T(8,128)S(1)} %get-tuple-element.31) | copy-start | bytes 1572868
  14.5 23.1 %copy-start.2 = (bf16[256,4096]{1,0:T(8,128)(2,1)S(1)}, bf16[256,4096]{1,0:T(8,128)(2,1)}, u32[]{:S(2)}) copy-start(bf16[256,4096]{1,0:T(8,128)(2,1)} %w.1) | copy-start | bytes 6291460
  14.5 23.1 %copy-start.3 = (bf16[128,4096]{1,0:T(8,128)(2,1)S(1)}, bf16[128,4096]{1,0:T(8,128)(2,1)}, u32[]{:S(2)}) copy-start(bf16[128,4096]{1,0:T(8,128)(2,1)} %skip.1) | copy-start | bytes 3145732
  14.5 23.1 %copy-start.6 = (f32[4096]{0:T(1024)S(1)}, f32[4096]{0:T(1024)}, u32[]{:S(2)}) copy-start(f32[4096]{0:T(1024)} %param.30) | copy-start | bytes 49156
  29.1 2.2 %copy-start.10 = (f32[16,64]{1,0:T(8,128)}, f32[16,64]{1,0:T(8,128)S(1)}, u32[]{:S(2)}) copy-start(f32[16,64]{1,0:T(8,128)S(1)} %mul.423) | copy-start | bytes 12292
  29.2 2.2 %copy-start.11 = (f32[16,64]{1,0:T(8,128)}, f32[16,64]{1,0:T(8,128)S(1)}, u32[]{:S(2)}) copy-start(f32[16,64]{1,0:T(8,128)S(1)} %mul.426) | copy-start | bytes 12292
  86.4 4.7 %copy-start.4 = (bf16[128,1024]{1,0:T(8,128)(2,1)}, bf16[128,1024]{1,0:T(8,128)(2,1)S(1)}, u32[]{:S(2)}) copy-start(bf16[128,1024]{1,0:T(8,128)(2,1)S(1)} %get-tuple-element.7) | copy-start | bytes 786436
  86.4 4.7 %copy-start.15 = (bf16[1,4096,512]{2,1,0:T(8,128)(2,1)S(1)}, bf16[1,4096,512]{2,1,0:T(8,128)(2,1)}, u32[]{:S(2)}) copy-start(bf16[1,4096,512]{2,1,0:T(8,128)(2,1)} %param.34) | copy-start | bytes 12582916
  91.1 2.7 %copy-start.13 = (f32[128,2]{0,1:T(2,128)S(1)}, f32[128,2]{0,1:T(2,128)}, u32[]{:S(2)}) copy-start(f32[128,2]{0,1:T(2,128)} %param.32) | copy-start | bytes 3076
  93.6 45.7 %copy-start.5 = (bf16[128,1024]{1,0:T(8,128)(2,1)S(1)}, bf16[128,1024]{1,0:T(8,128)(2,1)}, u32[]{:S(2)}) copy-start(bf16[128,1024]{1,0:T(8,128)(2,1)} %copy-done.4) | copy-start | bytes 786436
  94.1 2.2 %copy-start.1 = (bf16[1,512,4096]{2,1,0:T(8,128)(2,1)S(1)}, bf16[1,512,4096]{2,1,0:T(8,128)(2,1)}, u32[]{:S(2)}) copy-start(bf16[1,512,4096]{2,1,0:T(8,128)(2,1)} %param.35) | copy-start | bytes 12582916
